TPU v7x, 32 devices: a whole 2x2x4 slice. The times are simulated.
32 devices in a mesh: sp: 8 (over z, y), tp: 4 (over x, core).
Axes of the slice: x: 2, y: 2, z: 4, core: 2. Of those that a mesh axis runs over, the one named last changes fastest.
Arguments:
- cotangent: bfloat16 [1280, 2048], P('sp'), may hold values from -8 to 8
- saved_input: bfloat16 [1280, 2048], P('sp'), may hold values from -200 to 200
- routes: int32 [1280, 2], P('sp'), may hold values from 0 to 7, all different within a row; in each aligned block of 160 rows (0 to 159, 160 to 319, ...) at most 80 rows name the same one
- route_weight: float32 [1280, 2], P('sp'), may hold values from 0.2 to 1.5
- gate_proj: bfloat16 [8, 2048, 1024], P('sp', None, 'tp'), may hold values from -0.125 to 0.125
- up_proj: bfloat16 [8, 2048, 1024], P('sp', None, 'tp'), may hold values from -0.125 to 0.125
- down_proj: bfloat16 [8, 1024, 2048], P('sp', 'tp'), may hold values from -0.1875 to 0.1875
- out_proj: bfloat16 [2048, 1024], P(None, 'tp'), may hold values from -0.1875 to 0.1875
- conv_input: bfloat16 [1280, 1024], P('sp', 'tp'), may hold values from -6 to 6
- gate_branch: bfloat16 [1280, 1024], P('sp', 'tp'), may hold values from -6 to 6
- conv_taps: bfloat16 [4, 1024], P(None, 'tp'), may hold values from -3 to 3
- recur_map: bfloat16 [2, 16, 64, 64], P(None, 'tp'), may hold values from -0.75 to 0.75
- input_map: bfloat16 [2, 16, 64, 64], P(None, 'tp'), may hold values from -0.75 to 0.75
- decay_param: float32 [2, 1024], P(None, 'tp'), may hold values from 4 to 30
- decay_shift: float32 [2, 1280, 1024], P(None, 'sp', 'tp'), may hold values from -2 to 0, as said below
Outputs:
- grad_gate_proj: float32 [8, 2048, 1024], P('sp', None, 'tp')
- grad_up_proj: float32 [8, 2048, 1024], P('sp', None, 'tp')
- grad_down_proj: float32 [8, 1024, 2048], P('sp', 'tp')
- grad_out_proj: float32 [2048, 1024], P('sp', 'tp')
- grad_conv_input: bfloat16 [1280, 1024], P('sp', 'tp')
- grad_gate_branch: bfloat16 [1280, 1024], P('sp', 'tp')
Inputs may be any that keep to these rules, and one draw needn't show every extreme that they name: Each row names 2 different experts; among the rows of one device no expert is named by more than 80 rows, and in every draw some device routes exactly 80 rows to some expert. `decay_shift`: together with decay_param, -log_decay stays at or above softplus(-decay_param) for every channel and position.
All inputs are finite; a program needn't handle non-finite values.
Results may differ from a plain program's by a relative error of at most 0.013.
Values may be sent and summed in bfloat16 or wider, within the bound.
A program may use at most 128 MiB of HBM per device.

v0:
```python
import jax
import jax.numpy as jnp
from jax import lax
from jax.sharding import PartitionSpec as P

EPS = 1e-06
DECAY_SCALE = 8.0


def with_halo(block, sides, width):
    for axis, dim in sides:
        count = lax.axis_size(axis)
        forward = [(i, i + 1) for i in range(count - 1)]
        backward = [(target, source) for source, target in forward]
        low = lax.ppermute(
            lax.slice_in_dim(block, block.shape[dim] - width, None, axis=dim), axis, forward
        )
        high = lax.ppermute(lax.slice_in_dim(block, 0, width, axis=dim), axis, backward)
        block = jnp.concatenate([low, block, high], axis=dim)
    return block


def prefix(part, axis, combine, identity, reverse):
    count = lax.axis_size(axis)
    place = lax.axis_index(axis)
    ahead = count - 1 - place if reverse else place
    gathered = jax.tree.map(lambda a: lax.all_gather(a, axis), part)
    state = jax.tree.map(lambda a, e: jnp.zeros_like(a) + jnp.asarray(e, a.dtype), part, identity)

    def one(lap, state):
        source = count - 1 - lap if reverse else lap
        return combine(
            state, jax.tree.map(lambda a: lax.dynamic_index_in_dim(a, source, 0, False), gathered)
        )

    return lax.fori_loop(0, ahead, one, state)


def block_matrix(maps):
    heads = maps.shape[0]
    eye = jnp.eye(heads, dtype=jnp.float32)
    full = jnp.einsum("hij,hg->higj", maps.astype(jnp.float32), eye)
    return full.reshape(heads * maps.shape[1], heads * maps.shape[2])


def gate_terms(conv_out, recur_map, input_map, decay_param, decay_shift):
    recur = jax.nn.sigmoid(
        jnp.dot(conv_out, block_matrix(recur_map), precision=lax.Precision.HIGHEST)
    )
    inputs = jax.nn.sigmoid(
        jnp.dot(conv_out, block_matrix(input_map), precision=lax.Precision.HIGHEST)
    )
    log_decay = -DECAY_SCALE * recur * jax.nn.softplus(-decay_param)[None, :] + decay_shift
    decay = jnp.exp(log_decay)
    drive = jnp.sqrt(-jnp.expm1(2.0 * log_decay)) * (inputs * conv_out)
    return (decay, drive)


def link(earlier, later):
    return (earlier[0] * later[0], later[0] * earlier[1] + later[1])


def link_pairs(earlier, later):
    first = link((earlier[0], earlier[1]), (later[0], later[1]))
    second = link((earlier[2], earlier[3]), (later[2], later[3]))
    return first + second


def sweep(coef, drive, reverse):
    return lax.associative_scan(link, (coef, drive), axis=0, reverse=reverse)


def shards(
    cotangent,
    saved_input,
    routes,
    route_weight,
    gate_proj,
    up_proj,
    down_proj,
    out_proj,
    conv_input,
    gate_branch,
    conv_taps,
    recur_map,
    input_map,
    decay_param,
    decay_shift,
):
    length, width = cotangent.shape
    top = routes.shape[1]
    experts = lax.axis_size("sp") * gate_proj.shape[0]
    slots = 4 * length // lax.axis_size("sp")
    inputs32 = saved_input.astype(jnp.float32)
    inv_rms = lax.rsqrt(jnp.mean(inputs32 * inputs32, axis=1, keepdims=True) + EPS)
    normed = inputs32 * inv_rms
    expert_input = normed.astype(jnp.bfloat16)
    scaled = (route_weight[:, :, None] * cotangent.astype(jnp.float32)[:, None, :]).astype(
        jnp.bfloat16
    )
    scaled = scaled.reshape(length * top, width)
    flat_expert = routes.reshape(-1)
    onehot = (flat_expert[:, None] == jnp.arange(experts, dtype=jnp.int32)[None, :]).astype(
        jnp.int32
    )
    earlier_count = jnp.cumsum(onehot, axis=0) - onehot
    rank = jnp.sum(earlier_count * onehot, axis=1)
    target = flat_expert * slots + rank
    token_of = jnp.arange(length * top, dtype=jnp.int32) // top
    fourth = width // lax.axis_size("tp")
    first_col = lax.axis_index("tp") * fourth
    own_scaled = lax.dynamic_slice_in_dim(scaled, first_col, fourth, 1)
    own_input = lax.dynamic_slice_in_dim(expert_input, first_col, fourth, 1)
    send_scaled = jnp.zeros((experts * slots, fourth), jnp.bfloat16).at[target].set(own_scaled)
    send_input = (
        jnp.zeros((experts * slots, fourth), jnp.bfloat16).at[target].set(own_input[token_of])
    )
    part_scaled, part_input = (
        lax.all_to_all(
            send_scaled.reshape(experts, slots, fourth),
            "sp",
            split_axis=0,
            concat_axis=0,
            tiled=True,
        ),
        lax.all_to_all(
            send_input.reshape(experts, slots, fourth),
            "sp",
            split_axis=0,
            concat_axis=0,
            tiled=True,
        ),
    )
    got_scaled, got_input = (
        lax.all_gather(part_scaled, "tp", axis=2, tiled=True),
        lax.all_gather(part_input, "tp", axis=2, tiled=True),
    )
    rows_scaled = got_scaled.reshape(experts * slots, width)
    rows_input = got_input.reshape(experts * slots, width)
    w_gate = gate_proj[0]
    w_up = up_proj[0]
    w_down = down_proj[0]
    gate_pre = jnp.dot(rows_input, w_gate, preferred_element_type=jnp.float32)
    up_pre = jnp.dot(rows_input, w_up, preferred_element_type=jnp.float32)
    gate_sig = jax.nn.sigmoid(gate_pre)
    gate_act = gate_pre * gate_sig
    hidden = (gate_act * up_pre).astype(jnp.bfloat16)
    hidden_grad = lax.dot_general(
        rows_scaled, w_down, (((1,), (1,)), ((), ())), preferred_element_type=jnp.float32
    )
    gate_grad = (hidden_grad * up_pre * gate_sig * (1.0 + gate_pre * (1.0 - gate_sig))).astype(
        jnp.bfloat16
    )
    up_grad = (hidden_grad * gate_act).astype(jnp.bfloat16)
    grad_down = lax.dot_general(
        hidden, rows_scaled, (((0,), (0,)), ((), ())), preferred_element_type=jnp.float32
    )
    grad_gate = lax.dot_general(
        rows_input, gate_grad, (((0,), (0,)), ((), ())), preferred_element_type=jnp.float32
    )
    grad_up = lax.dot_general(
        rows_input, up_grad, (((0,), (0,)), ((), ())), preferred_element_type=jnp.float32
    )
    partial_rows = lax.dot_general(
        gate_grad, w_gate, (((1,), (1,)), ((), ())), preferred_element_type=jnp.float32
    )
    partial_rows = partial_rows + lax.dot_general(
        up_grad, w_up, (((1,), (1,)), ((), ())), preferred_element_type=jnp.float32
    )
    summed = lax.psum(partial_rows.astype(jnp.bfloat16), "tp")
    back = lax.all_to_all(
        summed.reshape(experts, slots, width), "sp", split_axis=0, concat_axis=0, tiled=True
    )
    routed = back.reshape(experts * slots, width)[target].reshape(length, top, width)
    normed_grad = jnp.sum(routed.astype(jnp.float32), axis=1)
    mixed_grad = cotangent.astype(jnp.float32) + inv_rms * (
        normed_grad - normed * jnp.mean(normed_grad * normed, axis=1, keepdims=True)
    )
    mixed_grad_b = mixed_grad.astype(jnp.bfloat16)
    taps32 = conv_taps.astype(jnp.float32)
    padded = with_halo(conv_input, (("sp", 0),), 2)
    conv_out = jnp.zeros((length, padded.shape[1]), jnp.float32)
    for offset in range(taps32.shape[0]):
        conv_out = conv_out + padded[offset : offset + length].astype(jnp.float32) * taps32[offset]
    (coef_f, drive_f), pull_f = jax.vjp(
        lambda value: gate_terms(value, recur_map[0], input_map[0], decay_param[0], decay_shift[0]),
        conv_out,
    )
    (coef_b, drive_b), pull_b = jax.vjp(
        lambda value: gate_terms(value, recur_map[1], input_map[1], decay_param[1], decay_shift[1]),
        conv_out,
    )
    out_grad = jnp.dot(mixed_grad_b, out_proj, preferred_element_type=jnp.float32)
    activated, pull_gelu = jax.vjp(jax.nn.gelu, gate_branch.astype(jnp.float32))
    carried = out_grad * activated
    cum_f, state_f0 = sweep(coef_f, drive_f, False)
    cum_bf, after_b0 = sweep(coef_b, coef_b * carried, False)
    cum_b, state_b0 = sweep(coef_b, drive_b, True)
    cum_fr, after_f0 = sweep(coef_f, coef_f * carried, True)
    ones = jnp.ones((conv_out.shape[1],), jnp.float32)
    zero_filled = jnp.zeros((conv_out.shape[1],), jnp.float32)
    lower = prefix(
        (cum_f[-1], state_f0[-1], cum_bf[-1], after_b0[-1]),
        "sp",
        link_pairs,
        (ones, zero_filled, ones, zero_filled),
        False,
    )
    upper = prefix(
        (cum_b[0], state_b0[0], cum_fr[0], after_f0[0]),
        "sp",
        link_pairs,
        (ones, zero_filled, ones, zero_filled),
        True,
    )
    state_f = state_f0 + cum_f * lower[1][None, :]
    after_b = after_b0 + cum_bf * lower[3][None, :]
    state_b = state_b0 + cum_b * upper[1][None, :]
    after_f = after_f0 + cum_fr * upper[3][None, :]
    adjoint_f = carried + jnp.concatenate([after_f[1:], upper[3][None, :]], axis=0)
    adjoint_b = carried + jnp.concatenate([lower[3][None, :], after_b[:-1]], axis=0)
    prev_f = jnp.concatenate([lower[1][None, :], state_f[:-1]], axis=0)
    next_b = jnp.concatenate([state_b[1:], upper[1][None, :]], axis=0)
    conv_grad = (
        pull_f((adjoint_f * prev_f, adjoint_f))[0] + pull_b((adjoint_b * next_b, adjoint_b))[0]
    )
    states = state_f + state_b
    mixed_out = (activated * states).astype(jnp.bfloat16)
    branch_grad = pull_gelu(out_grad * states)[0].astype(jnp.bfloat16)
    grad_out = lax.psum_scatter(
        lax.dot_general(
            mixed_grad_b, mixed_out, (((0,), (0,)), ((), ())), preferred_element_type=jnp.float32
        ),
        "sp",
        scatter_dimension=0,
        tiled=True,
    )
    grad_pad = with_halo(conv_grad.astype(jnp.bfloat16), (("sp", 0),), 2).astype(conv_grad.dtype)
    input_grad = jnp.zeros((length, conv_grad.shape[1]), jnp.float32)
    for offset in range(taps32.shape[0]):
        input_grad = input_grad + grad_pad[4 - offset : 4 - offset + length] * taps32[offset]
    return (
        grad_gate[None],
        grad_up[None],
        grad_down[None],
        grad_out,
        input_grad.astype(jnp.bfloat16),
        branch_grad,
    )


def solution(mesh):
    in_specs = (
        P("sp", None),
        P("sp", None),
        P("sp", None),
        P("sp", None),
        P("sp", None, "tp"),
        P("sp", None, "tp"),
        P("sp", "tp", None),
        P(None, "tp"),
        P("sp", "tp"),
        P("sp", "tp"),
        P(None, "tp"),
        P(None, "tp", None, None),
        P(None, "tp", None, None),
        P(None, "tp"),
        P(None, "sp", "tp"),
    )
    out_specs = (
        P("sp", None, "tp"),
        P("sp", None, "tp"),
        P("sp", "tp", None),
        P("sp", "tp"),
        P("sp", "tp"),
        P("sp", "tp"),
    )
    return jax.shard_map(shards, mesh=mesh, in_specs=in_specs, out_specs=out_specs, check_vma=False)
```

profile of v0, /device:TPU:0, one launch (start us, length us, event | category | flops | bytes accessed | tf_op | source)
XLA Modules:
  0.0 605.2 jit_solution(16723660355794471832)
XLA Ops:
  13.1 3.4 scatter_custom_fusion
  16.5 24.9 %all_to_all.15 = bf16[8,80,512]{2,1,0:T(8,128)(2,1)} all-to-all(bf16[8,80,512]{2,1,0:T(8,128)(2,1)S(1)} %bitcast.163), channel_id=1, replica_groups=mesh['sp'=8,'tp'=4] {'sp'}, dimensions={0} | all-to-all | bytes 1310720 | tf_op jit(solution)/shard_map/all_to_all | solution.py:126
  41.5 2.8 mul.742
  44.3 4.6 mul.743
  49.2 2.5 scatter_custom_fusion.1
  51.7 20.7 %all_to_all.16 = bf16[8,80,512]{2,1,0:T(8,128)(2,1)} all-to-all(bf16[8,80,512]{2,1,0:T(8,128)(2,1)S(1)} %bitcast.162), channel_id=1, replica_groups=mesh['sp'=8,'tp'=4] {'sp'}, dimensions={0} | all-to-all | bytes 1310720 | tf_op jit(solution)/shard_map/all_to_all | solution.py:119
  73.1 3.6 fusion.17
  78.4 18.4 %all-gather.13.cloned.1.call-done = bf16[8,80,2048]{2,1,0:T(8,128)(2,1)} async-done(((bf16[8,80,512]{2,1,0:T(8,128)(2,1)}), bf16[8,80,2048]{2,1,0:T(8,128)(2,1)}) %all-gather.13.cloned.1.call-update) | async-done | bytes 2621456 | tf_op jit(solution)/shard_map/all_gather | solution.py:135
  96.8 3.4 multiply_convert_fusion.1
  101.1 2.3 add_convert_fusion
  103.5 60.0 %all-reduce.115.cloned.1.call-done = bf16[8,80,2048]{2,1,0:T(8,128)(2,1)} async-done(((bf16[8,80,2048]{2,1,0:T(8,128)(2,1)}), bf16[8,80,2048]{2,1,0:T(8,128)(2,1)}) %all-reduce.115.cloned.1.call-update) | async-done | bytes 2621456 | tf_op jit(solution)/shard_map/psum | solution.py:170
  163.6 5.5 all-to-all-start.2
  169.1 3.9 collective-permute-start
  179.8 2.1 reshape.182
  186.0 4.2 collective-permute-done
  197.4 30.9 %all-to-all-done.2 = bf16[8,80,2048]{2,1,0:T(8,128)(2,1)S(1)} async-done(((bf16[8,80,2048]{2,1,0:T(8,128)(2,1)}), bf16[8,80,2048]{2,1,0:T(8,128)(2,1)S(1)}, u32[]{:S(2)}, u32[]{:S(2)}) %all-to-all-start.2) | async-done | bytes 2621472 | tf_op jit(solution)/shard_map/all_to_all | solution.py:171
  228.3 3.2 gather_fusion
  231.5 4.1 reshape.184
  235.5 5.0 reduce_sum.41
  332.4 22.5 %all-gather.4 = f32[8,1,256]{2,1,0:T(1,128)S(1)} all-gather(f32[1,1,256]{2,1,0:T(1,128)} %add_bitcast_fusion.4), channel_id=1, replica_groups=mesh['sp'=8,'tp'=4] {'sp'}, dimensions={0}, use_global_device_ids=true | all-gather | bytes 9216 | tf_op jit(solution)/shard_map/all_gather | solution.py:27
  354.9 17.1 %all-gather.5 = f32[8,1,256]{2,1,0:T(1,128)S(1)} all-gather(f32[1,1,256]{2,1,0:T(1,128)} %add_bitcast_fusion.3), channel_id=1, replica_groups=mesh['sp'=8,'tp'=4] {'sp'}, dimensions={0}, use_global_device_ids=true | all-gather | bytes 9216 | tf_op jit(solution)/shard_map/all_gather | solution.py:27
  380.0 17.7 %all-gather.6 = f32[8,1,256]{2,1,0:T(1,128)S(1)} all-gather(f32[1,1,256]{2,1,0:T(1,128)S(1)} %add_bitcast_fusion.2), channel_id=1, replica_groups=mesh['sp'=8,'tp'=4] {'sp'}, dimensions={0}, use_global_device_ids=true | all-gather | bytes 9216 | tf_op jit(solution)/shard_map/all_gather | solution.py:27
  398.5 16.9 %all-gather.7 = f32[8,1,256]{2,1,0:T(1,128)S(1)} all-gather(f32[1,1,256]{2,1,0:T(1,128)S(1)} %add_bitcast_fusion.1), channel_id=1, replica_groups=mesh['sp'=8,'tp'=4] {'sp'}, dimensions={0}, use_global_device_ids=true | all-gather | bytes 9216 | tf_op jit(solution)/shard_map/all_gather | solution.py:27
  426.7 17.6 %all-gather = f32[8,1,256]{2,1,0:T(1,128)S(1)} all-gather(f32[1,1,256]{2,1,0:T(1,128)S(1)} %add_bitcast_fusion.8), channel_id=1, replica_groups=mesh['sp'=8,'tp'=4] {'sp'}, dimensions={0}, use_global_device_ids=true | all-gather | bytes 9216 | tf_op jit(solution)/shard_map/all_gather | solution.py:27
  446.5 17.0 %all-gather.1 = f32[8,1,256]{2,1,0:T(1,128)S(1)} all-gather(f32[1,1,256]{2,1,0:T(1,128)S(1)} %add_bitcast_fusion.7), channel_id=1, replica_groups=mesh['sp'=8,'tp'=4] {'sp'}, dimensions={0}, use_global_device_ids=true | all-gather | bytes 9216 | tf_op jit(solution)/shard_map/all_gather | solution.py:27
  480.0 17.6 %all-gather.2 = f32[8,1,256]{2,1,0:T(1,128)S(1)} all-gather(f32[1,1,256]{2,1,0:T(1,128)S(1)} %add_bitcast_fusion.6), channel_id=1, replica_groups=mesh['sp'=8,'tp'=4] {'sp'}, dimensions={0}, use_global_device_ids=true | all-gather | bytes 9216 | tf_op jit(solution)/shard_map/all_gather | solution.py:27
  501.6 17.0 %all-gather.3 = f32[8,1,256]{2,1,0:T(1,128)S(1)} all-gather(f32[1,1,256]{2,1,0:T(1,128)S(1)} %add_bitcast_fusion.5), channel_id=1, replica_groups=mesh['sp'=8,'tp'=4] {'sp'}, dimensions={0}, use_global_device_ids=true | all-gather | bytes 9216 | tf_op jit(solution)/shard_map/all_gather | solution.py:27
  522.4 4.2 convolution_bitcast_fusion.2
  526.7 2.4 convolution_bitcast_fusion
  537.4 5.5 collective-permute-start.2
  542.9 2.3 convolution_bitcast_fusion.1
  546.0 52.5 %reduce-scatter.2.cloned.1.call-done = f32[256,256]{1,0:T(8,128)} async-done(((f32[2048,256]{1,0:T(8,128)}), f32[256,256]{1,0:T(8,128)}) %reduce-scatter.2.cloned.1.call-update) | async-done | bytes 262160 | tf_op jit(solution)/shard_map/reduce_scatter | solution.py:230
  (711 shorter events, 173.3 us)
Async XLA Ops:
  7.2 65.9 %copy-start = (bf16[1,2048,256]{2,1,0:T(8,128)(2,1)S(1)}, bf16[1,2048,256]{2,1,0:T(8,128)(2,1)}, u32[]{:S(2)}) copy-start(bf16[1,2048,256]{2,1,0:T(8,128)(2,1)} %param.23) | copy-start | bytes 3145732
  7.2 65.8 %all-gather.11.cloned.1.call-start = ((), (), s32[]{:S(2)}) async-start(), calls=%async_computation.4 | async-start | bytes 3276800 | tf_op jit(solution)/shard_map/all_gather | solution.py:136
  41.4 55.4 %all-gather.13.cloned.1.call-start = ((), (), s32[]{:S(2)}) async-start(), calls=%async_computation.5 | async-start | bytes 3276800 | tf_op jit(solution)/shard_map/all_gather | solution.py:135
  72.5 91.1 %all-reduce.115.cloned.1.call-start = ((), (), s32[]{:S(2)}) async-start(), calls=%async_computation.6 | async-start | bytes 5242880 | tf_op jit(solution)/shard_map/psum | solution.py:170
  103.5 65.6 %copy-start.38 = (bf16[160,256]{1,0:T(8,128)(2,1)S(1)}, bf16[160,256]{1,0:T(8,128)(2,1)}, u32[]{:S(2)}) copy-start(bf16[160,256]{1,0:T(8,128)(2,1)} %param.27) | copy-start | bytes 245764
  103.5 70.9 %copy-start.61 = (f32[2,256]{1,0:T(2,128)S(1)}, f32[2,256]{1,0:T(2,128)}, u32[]{:S(2)}) copy-start(f32[2,256]{1,0:T(2,128)} %param.32) | copy-start | bytes 6148
  103.5 71.5 %copy-start.53 = (bf16[4,256]{1,0:T(4,128)(2,1)S(1)}, bf16[4,256]{1,0:T(4,128)(2,1)}, u32[]{:S(2)}) copy-start(bf16[4,256]{1,0:T(4,128)(2,1)} %param.29) | copy-start | bytes 6148
  163.6 64.7 %all-to-all-start.2 = ((bf16[8,80,2048]{2,1,0:T(8,128)(2,1)}), bf16[8,80,2048]{2,1,0:T(8,128)(2,1)S(1)}, u32[]{:S(2)}, u32[]{:S(2)}) async-start(bf16[8,80,2048]{2,1,0:T(8,128)(2,1)} %all-reduce.115.cloned.1.call-done), calls=%async_computation.2 | async-start | bytes 5242880 | tf_op jit(solution)/shard_map/all_to_all | solution.py:171
  169.1 429.4 %reduce-scatter.2.cloned.1.call-start = ((), (), s32[]{:S(2)}) async-start(), calls=%async_computation.7 | async-start | bytes 2359296 | tf_op jit(solution)/shard_map/reduce_scatter | solution.py:230
  169.1 21.1 %collective-permute-start = (bf16[2,256]{1,0:T(2,128)(2,1)S(1)}, bf16[2,256]{1,0:T(2,128)(2,1)S(1)}, u32[]{:S(2)}, u32[]{:S(2)}) collective-permute-start(bf16[2,256]{1,0:T(2,128)(2,1)S(1)} %get-tuple-element.334), channel_id=1, source_target_pairs={{0,4},{4,8},{8,12},{12,16},{16,20},{20,24},{24,28},{1,5},{5,9},{9,... | collective-permute-start | bytes 3080 | tf_op jit(solution)/shard_map/ppermute | solution.py:15
  173.0 17.2 %collective-permute-start.1 = (bf16[2,256]{1,0:T(2,128)(2,1)S(1)}, bf16[2,256]{1,0:T(2,128)(2,1)S(1)}, u32[]{:S(2)}, u32[]{:S(2)}) collective-permute-start(bf16[2,256]{1,0:T(2,128)(2,1)S(1)} %get-tuple-element.333), channel_id=1, source_target_pairs={{4,0},{8,4},{12,8},{16,12},{20,16},{24,20},{28,24},{5,1},{9,5},{13... | collective-permute-start | bytes 3080 | tf_op jit(solution)/shard_map/ppermute | solution.py:18
  297.5 74.5 %copy-start.29 = (f32[79,256]{1,0:T(8,128)S(1)}, f32[79,256]{1,0:T(8,128)}, u32[]{:S(2)}) copy-start(f32[79,256]{1,0:T(8,128)} %slice.1206) | copy-start | bytes 242692
  308.4 70.4 %copy-start.36 = (f32[19,256]{1,0:T(8,128)S(1)}, f32[19,256]{1,0:T(8,128)}, u32[]{:S(2)}) copy-start(f32[19,256]{1,0:T(8,128)} %slice.1202) | copy-start | bytes 58372
  308.4 70.4 %copy-start.37 = (f32[19,256]{1,0:T(8,128)S(1)}, f32[19,256]{1,0:T(8,128)}, u32[]{:S(2)}) copy-start(f32[19,256]{1,0:T(8,128)} %slice.1167) | copy-start | bytes 58372
  313.8 65.7 %copy-start.57 = (f32[1,256]{1,0:T(1,128)S(1)}, f32[1,256]{1,0:T(1,128)}, u32[]{:S(2)}) copy-start(f32[1,256]{1,0:T(1,128)} %slice.1353) | copy-start | bytes 3076
  313.8 65.7 %copy-start.32 = (f32[39,256]{1,0:T(8,128)S(1)}, f32[39,256]{1,0:T(8,128)}, u32[]{:S(2)}) copy-start(f32[39,256]{1,0:T(8,128)} %slice.1204) | copy-start | bytes 119812
  313.8 65.7 %copy-start.33 = (f32[39,256]{1,0:T(8,128)S(1)}, f32[39,256]{1,0:T(8,128)}, u32[]{:S(2)}) copy-start(f32[39,256]{1,0:T(8,128)} %slice.1169) | copy-start | bytes 119812
  313.9 65.7 %copy-start.60 = (f32[1,256]{1,0:T(1,128)S(1)}, f32[1,256]{1,0:T(1,128)}, u32[]{:S(2)}) copy-start(f32[1,256]{1,0:T(1,128)} %slice.1352) | copy-start | bytes 3076
  315.3 64.5 %copy-start.59 = (f32[1,256]{1,0:T(1,128)S(1)}, f32[1,256]{1,0:T(1,128)}, u32[]{:S(2)}) copy-start(f32[1,256]{1,0:T(1,128)} %slice.1372) | copy-start | bytes 3076
  328.6 51.3 %copy-start.56 = (f32[1,256]{1,0:T(1,128)S(1)}, f32[1,256]{1,0:T(1,128)}, u32[]{:S(2)}) copy-start(f32[1,256]{1,0:T(1,128)} %get-tuple-element.310) | copy-start | bytes 3076
  379.5 43.5 %copy-start.34 = (f32[19,256]{1,0:T(8,128)S(1)}, f32[19,256]{1,0:T(8,128)}, u32[]{:S(2)}) copy-start(f32[19,256]{1,0:T(8,128)} %slice.986) | copy-start | bytes 58372
  379.7 44.7 %copy-start.30 = (f32[39,256]{1,0:T(8,128)S(1)}, f32[39,256]{1,0:T(8,128)}, u32[]{:S(2)}) copy-start(f32[39,256]{1,0:T(8,128)} %slice.988) | copy-start | bytes 119812
  379.7 44.7 %copy-start.31 = (f32[39,256]{1,0:T(8,128)S(1)}, f32[39,256]{1,0:T(8,128)}, u32[]{:S(2)}) copy-start(f32[39,256]{1,0:T(8,128)} %slice.948) | copy-start | bytes 119812
  379.9 45.3 %copy-start.58 = (f32[1,256]{1,0:T(1,128)S(1)}, f32[1,256]{1,0:T(1,128)}, u32[]{:S(2)}) copy-start(f32[1,256]{1,0:T(1,128)} %slice.1232) | copy-start | bytes 3076
  379.9 46.0 %copy-start.27 = (f32[79,256]{1,0:T(8,128)S(1)}, f32[79,256]{1,0:T(8,128)}, u32[]{:S(2)}) copy-start(f32[79,256]{1,0:T(8,128)} %slice.990) | copy-start | bytes 242692
  379.9 46.0 %copy-start.28 = (f32[79,256]{1,0:T(8,128)S(1)}, f32[79,256]{1,0:T(8,128)}, u32[]{:S(2)}) copy-start(f32[79,256]{1,0:T(8,128)} %slice.942) | copy-start | bytes 242692
  398.5 47.3 %copy-start.15 = (f32[160,256]{1,0:T(8,128)}, f32[160,256]{1,0:T(8,128)S(1)}, u32[]{:S(2)}) copy-start(f32[160,256]{1,0:T(8,128)S(1)} %pad.459) | copy-start | bytes 491524
  416.8 47.3 %copy-start.54 = (f32[2,256]{1,0:T(2,128)S(1)}, f32[2,256]{1,0:T(2,128)}, u32[]{:S(2)}) copy-start(f32[2,256]{1,0:T(2,128)} %slice.1057) | copy-start | bytes 6148
  416.8 47.3 %copy-start.55 = (f32[2,256]{1,0:T(2,128)S(1)}, f32[2,256]{1,0:T(2,128)}, u32[]{:S(2)}) copy-start(f32[2,256]{1,0:T(2,128)} %slice.1056) | copy-start | bytes 6148
  536.0 9.2 %collective-permute-start.3 = (bf16[2,256]{1,0:T(2,128)(2,1)S(1)}, bf16[2,256]{1,0:T(2,128)(2,1)S(1)}, u32[]{:S(2)}, u32[]{:S(2)}) collective-permute-start(bf16[2,256]{1,0:T(2,128)(2,1)S(1)} %get-tuple-element.316), channel_id=1, source_target_pairs={{4,0},{8,4},{12,8},{16,12},{20,16},{24,20},{28,24},{5,1},{9,5},{13... | collective-permute-start | bytes 3080 | tf_op jit(solution)/shard_map/ppermute | solution.py:18
  537.3 61.1 %copy-start.1 = (bf16[1,2048,256]{2,1,0:T(8,128)(2,1)S(1)}, bf16[1,2048,256]{2,1,0:T(8,128)(2,1)}, u32[]{:S(2)}) copy-start(bf16[1,2048,256]{2,1,0:T(8,128)(2,1)} %param.23) | copy-start | bytes 3145732
  537.4 7.8 %collective-permute-start.2 = (bf16[2,256]{1,0:T(2,128)(2,1)S(1)}, bf16[2,256]{1,0:T(2,128)(2,1)S(1)}, u32[]{:S(2)}, u32[]{:S(2)}) collective-permute-start(bf16[2,256]{1,0:T(2,128)(2,1)S(1)} %get-tuple-element.315), channel_id=1, source_target_pairs={{0,4},{4,8},{8,12},{12,16},{16,20},{20,24},{24,28},{1,5},{5,9},{9,... | collective-permute-start | bytes 3080 | tf_op jit(solution)/shard_map/ppermute | solution.py:15
  (47 other events, 377.7 us)
Sparse Core Ops, SparseCore 0:
  41.6 24.1 all-gather.10
  72.6 24.1 all-gather.12
  103.6 59.8 all-reduce.114
  522.5 75.9 reduce-scatter.1
where the time goes:
time: 616 us; the launch traced here: 605 us
  blocking collectives  189 us (31%)
  waiting for transfers between devices  166 us (27%)
  local copies, waits for them, and re-layouts  118 us (19%)
  other arithmetic  64.7 us (11%)
  matrix products  32.2 us (5%)
  starting transfers between devices  18.1 us (3%)
  between operations  16.6 us (3%)
    all_gather x8, blocking collectives, prefix(): gathered = jax.tree.map(lambda a: lax.all_gather(a, axis), part)  143 us
    slice x198, local copies, waits for them, and re-layouts, sweep(): return lax.associative_scan(link, (coef, drive), axis=0, reverse=reverse)  76.2 us
    psum x1, waiting for transfers between devices, shards(): summed = lax.psum(partial_rows.astype(jnp.bfloat16), 'tp')  60 us
    reduce_scatter x1, waiting for transfers between devices, shards(): lax.psum_scatter(lax.dot_general(mixed_grad_b, mixed_out, (((0,), (0,)),...  52.5 us
    all_to_all x1, waiting for transfers between devices, shards(): lax.all_to_all(summed.reshape(experts, slots, width), 'sp', split_axis=0,...  30.9 us
    all_to_all x1, blocking collectives, shards(): lax.all_to_all(send_input.reshape(experts, slots, fourth), 'sp', split_ax...  24.9 us
    concatenate x48, other arithmetic, sweep(): return lax.associative_scan(link, (coef, drive), axis=0, reverse=reverse)  20.9 us
    all_to_all x1, blocking collectives, shards(): lax.all_to_all(send_scaled.reshape(experts, slots, fourth), 'sp', split_a...  20.7 us
  transfers between devices with their start and end apart: 9, of which 5 were waited for; matrix products, arithmetic and copies ran while one was open for 8% of the time, Pallas kernels for 0%

commit v1 on v0

--- a/solution.py
+++ b/solution.py
@@ -167,7 +167,7 @@
     partial_rows = partial_rows + lax.dot_general(
         up_grad, w_up, (((1,), (1,)), ((), ())), preferred_element_type=jnp.float32
     )
-    summed = lax.psum(partial_rows.astype(jnp.bfloat16), "tp")
+    summed = jnp.sum(lax.all_gather(partial_rows.astype(jnp.bfloat16), "tp"), axis=0)
     back = lax.all_to_all(
         summed.reshape(experts, slots, width), "sp", split_axis=0, concat_axis=0, tiled=True
     )

time: 616 us -> 635 us (1.031)
  waiting for transfers between devices: 166 us -> 177 us
  other arithmetic: 64.7 us -> 73.4 us
    all_gather x0 -> x1, waiting for transfers between devices: none -> 70.3 us  [shards(): lax.all_gather(partial_rows.astype(jnp.bfloat16), 'tp')]
    psum x1 -> x0, waiting for transfers between devices: 60 us -> none  [shards(): summed = lax.psum(partial_rows.astype(jnp.bfloat16), 'tp')]
    reduce_sum x0 -> x1, other arithmetic: none -> 8.71 us  [shards(): jnp.sum(lax.all_gather(partial_rows.astype(jnp.bfloat16), 'tp'), axis=0)]
where the time goes in v1:
time: 635 us; the launch traced here: 625 us
  blocking collectives  189 us (30%)
  waiting for transfers between devices  177 us (28%)
  local copies, waits for them, and re-layouts  118 us (19%)
  other arithmetic  73.4 us (12%)
  matrix products  32.1 us (5%)
  starting transfers between devices  18.2 us (3%)
  between operations  16.5 us (3%)
    all_gather x8, blocking collectives, prefix(): gathered = jax.tree.map(lambda a: lax.all_gather(a, axis), part)  143 us
    slice x198, local copies, waits for them, and re-layouts, sweep(): return lax.associative_scan(link, (coef, drive), axis=0, reverse=reverse)  76.3 us
    all_gather x1, waiting for transfers between devices, shards(): lax.all_gather(partial_rows.astype(jnp.bfloat16), 'tp')  70.3 us
    reduce_scatter x1, waiting for transfers between devices, shards(): lax.psum_scatter(lax.dot_general(mixed_grad_b, mixed_out, (((0,), (0,)),...  52.3 us
    all_to_all x1, waiting for transfers between devices, shards(): lax.all_to_all(summed.reshape(experts, slots, width), 'sp', split_axis=0,...  30.9 us
    all_to_all x1, blocking collectives, shards(): lax.all_to_all(send_input.reshape(experts, slots, fourth), 'sp', split_ax...  24.9 us
    concatenate x48, other arithmetic, sweep(): return lax.associative_scan(link, (coef, drive), axis=0, reverse=reverse)  20.8 us
    all_to_all x1, blocking collectives, shards(): lax.all_to_all(send_scaled.reshape(experts, slots, fourth), 'sp', split_a...  20.7 us
  transfers between devices with their start and end apart: 9, of which 5 were waited for; matrix products, arithmetic and copies ran while one was open for 8% of the time, Pallas kernels for 0%

profile of v1, /device:TPU:0, one launch (start us, length us, event | category | flops | bytes accessed | tf_op | source)
XLA Modules:
  0.0 624.7 jit_solution(16748103148402855600)
XLA Ops:
  13.1 3.4 scatter_custom_fusion
  16.5 24.9 %all_to_all.15 = bf16[8,80,512]{2,1,0:T(8,128)(2,1)} all-to-all(bf16[8,80,512]{2,1,0:T(8,128)(2,1)S(1)} %bitcast.165), channel_id=1, replica_groups=mesh['sp'=8,'tp'=4] {'sp'}, dimensions={0} | all-to-all | bytes 1310720 | tf_op jit(solution)/shard_map/all_to_all | solution.py:126
  41.5 2.8 mul.742
  44.3 4.6 mul.743
  49.2 2.5 scatter_custom_fusion.1
  51.7 20.7 %all_to_all.16 = bf16[8,80,512]{2,1,0:T(8,128)(2,1)} all-to-all(bf16[8,80,512]{2,1,0:T(8,128)(2,1)S(1)} %bitcast.164), channel_id=1, replica_groups=mesh['sp'=8,'tp'=4] {'sp'}, dimensions={0} | all-to-all | bytes 1310720 | tf_op jit(solution)/shard_map/all_to_all | solution.py:119
  73.0 3.6 fusion.17
  78.3 18.5 %all-gather.15.cloned.1.call-done = bf16[8,80,2048]{2,1,0:T(8,128)(2,1)} async-done(((bf16[8,80,512]{2,1,0:T(8,128)(2,1)}), bf16[8,80,2048]{2,1,0:T(8,128)(2,1)}) %all-gather.15.cloned.1.call-update) | async-done | bytes 2621456 | tf_op jit(solution)/shard_map/all_gather | solution.py:135
  96.8 3.4 multiply_convert_fusion.1
  101.1 2.4 add_convert_fusion
  103.5 70.3 %all-gather.17.cloned.1.call-done = bf16[2560,2048]{1,0:T(8,128)(2,1)} async-done(((bf16[640,2048]{1,0:T(8,128)(2,1)}), bf16[2560,2048]{1,0:T(8,128)(2,1)}) %all-gather.17.cloned.1.call-update) | async-done | bytes 10485776 | tf_op jit(solution)/shard_map/all_gather | solution.py:170
  173.8 8.7 %reduce_sum.53 = bf16[640,2048]{1,0:T(8,128)(2,1)} reduce(bf16[4,640,2048]{2,1,0:T(8,128)(2,1)} %bitcast.163, bf16[]{:T(256)} %constant.111.clone.1), dimensions={0}, to_apply=%region_6.7 | reduce | flops 3932160 | bytes 13107202 | tf_op jit(solution)/shard_map/reduce_sum | solution.py:170
  182.5 5.6 all-to-all-start.2
  188.2 3.9 collective-permute-start
  205.1 4.8 collective-permute-done
  217.2 30.9 %all-to-all-done.2 = bf16[8,80,2048]{2,1,0:T(8,128)(2,1)S(1)} async-done(((bf16[8,80,2048]{2,1,0:T(8,128)(2,1)}), bf16[8,80,2048]{2,1,0:T(8,128)(2,1)S(1)}, u32[]{:S(2)}, u32[]{:S(2)}) %all-to-all-start.2) | async-done | bytes 2621472 | tf_op jit(solution)/shard_map/all_to_all | solution.py:171
  248.0 3.2 gather_fusion
  251.2 4.0 reshape.184
  255.3 5.0 reduce_sum.54
  352.2 22.5 %all-gather.5 = f32[8,1,256]{2,1,0:T(1,128)S(1)} all-gather(f32[1,1,256]{2,1,0:T(1,128)} %add_bitcast_fusion.4), channel_id=1, replica_groups=mesh['sp'=8,'tp'=4] {'sp'}, dimensions={0}, use_global_device_ids=true | all-gather | bytes 9216 | tf_op jit(solution)/shard_map/all_gather | solution.py:27
  374.7 17.1 %all-gather.6 = f32[8,1,256]{2,1,0:T(1,128)S(1)} all-gather(f32[1,1,256]{2,1,0:T(1,128)} %add_bitcast_fusion.3), channel_id=1, replica_groups=mesh['sp'=8,'tp'=4] {'sp'}, dimensions={0}, use_global_device_ids=true | all-gather | bytes 9216 | tf_op jit(solution)/shard_map/all_gather | solution.py:27
  399.7 17.7 %all-gather.7 = f32[8,1,256]{2,1,0:T(1,128)S(1)} all-gather(f32[1,1,256]{2,1,0:T(1,128)S(1)} %add_bitcast_fusion.2), channel_id=1, replica_groups=mesh['sp'=8,'tp'=4] {'sp'}, dimensions={0}, use_global_device_ids=true | all-gather | bytes 9216 | tf_op jit(solution)/shard_map/all_gather | solution.py:27
  418.2 16.9 %all-gather.8 = f32[8,1,256]{2,1,0:T(1,128)S(1)} all-gather(f32[1,1,256]{2,1,0:T(1,128)S(1)} %add_bitcast_fusion.1), channel_id=1, replica_groups=mesh['sp'=8,'tp'=4] {'sp'}, dimensions={0}, use_global_device_ids=true | all-gather | bytes 9216 | tf_op jit(solution)/shard_map/all_gather | solution.py:27
  446.5 17.6 %all-gather.1 = f32[8,1,256]{2,1,0:T(1,128)S(1)} all-gather(f32[1,1,256]{2,1,0:T(1,128)S(1)} %add_bitcast_fusion.8), channel_id=1, replica_groups=mesh['sp'=8,'tp'=4] {'sp'}, dimensions={0}, use_global_device_ids=true | all-gather | bytes 9216 | tf_op jit(solution)/shard_map/all_gather | solution.py:27
  466.3 17.0 %all-gather.2 = f32[8,1,256]{2,1,0:T(1,128)S(1)} all-gather(f32[1,1,256]{2,1,0:T(1,128)S(1)} %add_bitcast_fusion.7), channel_id=1, replica_groups=mesh['sp'=8,'tp'=4] {'sp'}, dimensions={0}, use_global_device_ids=true | all-gather | bytes 9216 | tf_op jit(solution)/shard_map/all_gather | solution.py:27
  499.8 17.6 %all-gather.3 = f32[8,1,256]{2,1,0:T(1,128)S(1)} all-gather(f32[1,1,256]{2,1,0:T(1,128)S(1)} %add_bitcast_fusion.6), channel_id=1, replica_groups=mesh['sp'=8,'tp'=4] {'sp'}, dimensions={0}, use_global_device_ids=true | all-gather | bytes 9216 | tf_op jit(solution)/shard_map/all_gather | solution.py:27
  521.3 17.0 %all-gather.4 = f32[8,1,256]{2,1,0:T(1,128)S(1)} all-gather(f32[1,1,256]{2,1,0:T(1,128)S(1)} %add_bitcast_fusion.5), channel_id=1, replica_groups=mesh['sp'=8,'tp'=4] {'sp'}, dimensions={0}, use_global_device_ids=true | all-gather | bytes 9216 | tf_op jit(solution)/shard_map/all_gather | solution.py:27
  542.1 4.2 convolution_bitcast_fusion.2
  546.4 2.4 convolution_bitcast_fusion
  557.1 5.5 collective-permute-start.2
  562.6 2.3 convolution_bitcast_fusion.1
  565.7 52.3 %reduce-scatter.2.cloned.1.call-done = f32[256,256]{1,0:T(8,128)} async-done(((f32[2048,256]{1,0:T(8,128)}), f32[256,256]{1,0:T(8,128)}) %reduce-scatter.2.cloned.1.call-update) | async-done | bytes 262160 | tf_op jit(solution)/shard_map/reduce_scatter | solution.py:230
  (712 shorter events, 175.3 us)
Async XLA Ops:
  7.2 65.8 %copy-start = (bf16[1,2048,256]{2,1,0:T(8,128)(2,1)S(1)}, bf16[1,2048,256]{2,1,0:T(8,128)(2,1)}, u32[]{:S(2)}) copy-start(bf16[1,2048,256]{2,1,0:T(8,128)(2,1)} %param.23) | copy-start | bytes 3145732
  7.2 65.8 %all-gather.13.cloned.1.call-start = ((), (), s32[]{:S(2)}) async-start(), calls=%async_computation.4 | async-start | bytes 3276800 | tf_op jit(solution)/shard_map/all_gather | solution.py:136
  41.4 55.3 %all-gather.15.cloned.1.call-start = ((), (), s32[]{:S(2)}) async-start(), calls=%async_computation.5 | async-start | bytes 3276800 | tf_op jit(solution)/shard_map/all_gather | solution.py:135
  72.5 101.3 %all-gather.17.cloned.1.call-start = ((), (), s32[]{:S(2)}) async-start(), calls=%async_computation.7 | async-start | bytes 13107200 | tf_op jit(solution)/shard_map/all_gather | solution.py:170
  182.5 65.5 %all-to-all-start.2 = ((bf16[8,80,2048]{2,1,0:T(8,128)(2,1)}), bf16[8,80,2048]{2,1,0:T(8,128)(2,1)S(1)}, u32[]{:S(2)}, u32[]{:S(2)}) async-start(bf16[8,80,2048]{2,1,0:T(8,128)(2,1)} %bitcast.162), calls=%async_computation.2 | async-start | bytes 5242880 | tf_op jit(solution)/shard_map/all_to_all | solution.py:171
  188.1 429.8 %reduce-scatter.2.cloned.1.call-start = ((), (), s32[]{:S(2)}) async-start(), calls=%async_computation.6 | async-start | bytes 2359296 | tf_op jit(solution)/shard_map/reduce_scatter | solution.py:230
  188.2 21.7 %collective-permute-start = (bf16[2,256]{1,0:T(2,128)(2,1)S(1)}, bf16[2,256]{1,0:T(2,128)(2,1)S(1)}, u32[]{:S(2)}, u32[]{:S(2)}) collective-permute-start(bf16[2,256]{1,0:T(2,128)(2,1)S(1)} %get-tuple-element.334), channel_id=1, source_target_pairs={{0,4},{4,8},{8,12},{12,16},{16,20},{20,24},{24,28},{1,5},{5,9},{9,... | collective-permute-start | bytes 3080 | tf_op jit(solution)/shard_map/ppermute | solution.py:15
  192.1 17.8 %collective-permute-start.1 = (bf16[2,256]{1,0:T(2,128)(2,1)S(1)}, bf16[2,256]{1,0:T(2,128)(2,1)S(1)}, u32[]{:S(2)}, u32[]{:S(2)}) collective-permute-start(bf16[2,256]{1,0:T(2,128)(2,1)S(1)} %get-tuple-element.333), channel_id=1, source_target_pairs={{4,0},{8,4},{12,8},{16,12},{20,16},{24,20},{28,24},{5,1},{9,5},{13... | collective-permute-start | bytes 3080 | tf_op jit(solution)/shard_map/ppermute | solution.py:18
  317.3 74.5 %copy-start.29 = (f32[79,256]{1,0:T(8,128)S(1)}, f32[79,256]{1,0:T(8,128)}, u32[]{:S(2)}) copy-start(f32[79,256]{1,0:T(8,128)} %slice.1206) | copy-start | bytes 242692
  328.5 70.0 %copy-start.36 = (f32[19,256]{1,0:T(8,128)S(1)}, f32[19,256]{1,0:T(8,128)}, u32[]{:S(2)}) copy-start(f32[19,256]{1,0:T(8,128)} %slice.1202) | copy-start | bytes 58372
  328.5 70.0 %copy-start.37 = (f32[19,256]{1,0:T(8,128)S(1)}, f32[19,256]{1,0:T(8,128)}, u32[]{:S(2)}) copy-start(f32[19,256]{1,0:T(8,128)} %slice.1167) | copy-start | bytes 58372
  333.7 65.5 %copy-start.57 = (f32[1,256]{1,0:T(1,128)S(1)}, f32[1,256]{1,0:T(1,128)}, u32[]{:S(2)}) copy-start(f32[1,256]{1,0:T(1,128)} %slice.1353) | copy-start | bytes 3076
  333.8 65.5 %copy-start.32 = (f32[39,256]{1,0:T(8,128)S(1)}, f32[39,256]{1,0:T(8,128)}, u32[]{:S(2)}) copy-start(f32[39,256]{1,0:T(8,128)} %slice.1204) | copy-start | bytes 119812
  333.8 65.5 %copy-start.33 = (f32[39,256]{1,0:T(8,128)S(1)}, f32[39,256]{1,0:T(8,128)}, u32[]{:S(2)}) copy-start(f32[39,256]{1,0:T(8,128)} %slice.1169) | copy-start | bytes 119812
  333.8 65.5 %copy-start.60 = (f32[1,256]{1,0:T(1,128)S(1)}, f32[1,256]{1,0:T(1,128)}, u32[]{:S(2)}) copy-start(f32[1,256]{1,0:T(1,128)} %slice.1352) | copy-start | bytes 3076
  335.3 64.3 %copy-start.59 = (f32[1,256]{1,0:T(1,128)S(1)}, f32[1,256]{1,0:T(1,128)}, u32[]{:S(2)}) copy-start(f32[1,256]{1,0:T(1,128)} %slice.1372) | copy-start | bytes 3076
  348.4 51.2 %copy-start.56 = (f32[1,256]{1,0:T(1,128)S(1)}, f32[1,256]{1,0:T(1,128)}, u32[]{:S(2)}) copy-start(f32[1,256]{1,0:T(1,128)} %get-tuple-element.310) | copy-start | bytes 3076
  397.8 42.9 %copy-start.40 = (f32[9,256]{1,0:T(8,128)S(1)}, f32[9,256]{1,0:T(8,128)}, u32[]{:S(2)}) copy-start(f32[9,256]{1,0:T(8,128)} %slice.984) | copy-start | bytes 27652
  399.2 43.6 %copy-start.34 = (f32[19,256]{1,0:T(8,128)S(1)}, f32[19,256]{1,0:T(8,128)}, u32[]{:S(2)}) copy-start(f32[19,256]{1,0:T(8,128)} %slice.986) | copy-start | bytes 58372
  399.3 43.6 %copy-start.35 = (f32[19,256]{1,0:T(8,128)S(1)}, f32[19,256]{1,0:T(8,128)}, u32[]{:S(2)}) copy-start(f32[19,256]{1,0:T(8,128)} %slice.954) | copy-start | bytes 58372
  399.4 44.9 %copy-start.30 = (f32[39,256]{1,0:T(8,128)S(1)}, f32[39,256]{1,0:T(8,128)}, u32[]{:S(2)}) copy-start(f32[39,256]{1,0:T(8,128)} %slice.988) | copy-start | bytes 119812
  399.4 44.9 %copy-start.31 = (f32[39,256]{1,0:T(8,128)S(1)}, f32[39,256]{1,0:T(8,128)}, u32[]{:S(2)}) copy-start(f32[39,256]{1,0:T(8,128)} %slice.948) | copy-start | bytes 119812
  399.6 45.4 %copy-start.58 = (f32[1,256]{1,0:T(1,128)S(1)}, f32[1,256]{1,0:T(1,128)}, u32[]{:S(2)}) copy-start(f32[1,256]{1,0:T(1,128)} %slice.1232) | copy-start | bytes 3076
  399.6 46.1 %copy-start.27 = (f32[79,256]{1,0:T(8,128)S(1)}, f32[79,256]{1,0:T(8,128)}, u32[]{:S(2)}) copy-start(f32[79,256]{1,0:T(8,128)} %slice.990) | copy-start | bytes 242692
  399.7 46.1 %copy-start.28 = (f32[79,256]{1,0:T(8,128)S(1)}, f32[79,256]{1,0:T(8,128)}, u32[]{:S(2)}) copy-start(f32[79,256]{1,0:T(8,128)} %slice.942) | copy-start | bytes 242692
  418.2 47.5 %copy-start.15 = (f32[160,256]{1,0:T(8,128)}, f32[160,256]{1,0:T(8,128)S(1)}, u32[]{:S(2)}) copy-start(f32[160,256]{1,0:T(8,128)S(1)} %pad.459) | copy-start | bytes 491524
  436.5 47.4 %copy-start.54 = (f32[2,256]{1,0:T(2,128)S(1)}, f32[2,256]{1,0:T(2,128)}, u32[]{:S(2)}) copy-start(f32[2,256]{1,0:T(2,128)} %slice.1057) | copy-start | bytes 6148
  436.5 47.4 %copy-start.55 = (f32[2,256]{1,0:T(2,128)S(1)}, f32[2,256]{1,0:T(2,128)}, u32[]{:S(2)}) copy-start(f32[2,256]{1,0:T(2,128)} %slice.1056) | copy-start | bytes 6148
  495.3 43.1 %copy-start.17 = (f32[160,256]{1,0:T(8,128)}, f32[160,256]{1,0:T(8,128)S(1)}, u32[]{:S(2)}) copy-start(f32[160,256]{1,0:T(8,128)S(1)} %pad.390) | copy-start | bytes 491524
  555.7 9.2 %collective-permute-start.3 = (bf16[2,256]{1,0:T(2,128)(2,1)S(1)}, bf16[2,256]{1,0:T(2,128)(2,1)S(1)}, u32[]{:S(2)}, u32[]{:S(2)}) collective-permute-start(bf16[2,256]{1,0:T(2,128)(2,1)S(1)} %get-tuple-element.316), channel_id=1, source_target_pairs={{4,0},{8,4},{12,8},{16,12},{20,16},{24,20},{28,24},{5,1},{9,5},{13... | collective-permute-start | bytes 3080 | tf_op jit(solution)/shard_map/ppermute | solution.py:18
  557.0 61.0 %copy-start.1 = (bf16[1,2048,256]{2,1,0:T(8,128)(2,1)S(1)}, bf16[1,2048,256]{2,1,0:T(8,128)(2,1)}, u32[]{:S(2)}) copy-start(bf16[1,2048,256]{2,1,0:T(8,128)(2,1)} %param.23) | copy-start | bytes 3145732
  557.1 7.8 %collective-permute-start.2 = (bf16[2,256]{1,0:T(2,128)(2,1)S(1)}, bf16[2,256]{1,0:T(2,128)(2,1)S(1)}, u32[]{:S(2)}, u32[]{:S(2)}) collective-permute-start(bf16[2,256]{1,0:T(2,128)(2,1)S(1)} %get-tuple-element.315), channel_id=1, source_target_pairs={{0,4},{4,8},{8,12},{12,16},{16,20},{20,24},{24,28},{1,5},{5,9},{9,... | collective-permute-start | bytes 3080 | tf_op jit(solution)/shard_map/ppermute | solution.py:15
  (47 other events, 279.2 us)
Sparse Core Ops, SparseCore 0:
  41.6 24.1 all-gather.12
  72.6 24.1 all-gather.14
  103.6 70.1 all-gather.16
  542.2 75.7 reduce-scatter.1
